TPU v7x, 256 devices: a whole 4x4x8 slice. The times are simulated.
256 devices in a mesh: fs: 32 (over z, x), tp: 8 (over y, core).
Axes of the slice: x: 4, y: 4, z: 8, core: 2. Of those that a mesh axis runs over, the one named last changes fastest.
Arguments:
- later_rows: bfloat16 [32768, 2048], P(('fs', 'tp')), may hold values from -6 to 6
- earlier_rows: bfloat16 [32768, 2048], P(('fs', 'tp')), may hold values from -6 to 6
- cotangent: bfloat16 [32768, 2048], P(('fs', 'tp')), may hold values from -24 to 24
- up_weight: bfloat16 [2048, 4096], P('fs', 'tp'), may hold values from -0.125 to 0.125
- down_weight: bfloat16 [2048, 4096], P('fs', 'tp'), may hold values from -0.09375 to 0.09375
- up_total: float32 [2048, 4096], P('fs', 'tp'), may hold values from -6 to 6
- down_total: float32 [2048, 4096], P('fs', 'tp'), may hold values from -6 to 6
Outputs:
- later_out: bfloat16 [32768, 2048], P(('fs', 'tp'))
- earlier_grad: bfloat16 [32768, 2048], P(('fs', 'tp'))
- up_updated: float32 [2048, 4096], P('fs', 'tp')
- down_updated: float32 [2048, 4096], P('fs', 'tp')
All inputs are finite; a program needn't handle non-finite values.
Results may differ from a plain program's by a relative error of at most 0.015.
Values may be sent and summed in bfloat16 or wider, within the bound.
No kernel may reach another device: no remote copies, remote signals or barrier semaphores. Data moves between devices by JAX's collectives and lax.ppermute only.
A program may use at most 128 MiB of HBM per device.

v0:
```python
import math
import jax
import jax.numpy as jnp
from jax import lax
from jax.sharding import Mesh
from jax.sharding import PartitionSpec as P

FS = ("fs_0", "fs_1")
FS_TP = ("fs_0", "fs_1", "tp")


def side_by_side(arrays, axis, dim, along):
    ends, at = ([], 0)
    for a in arrays[:-1]:
        at += a.shape[along]
        ends.append(at)
    both = jnp.concatenate(arrays, axis=along)
    return tuple(jnp.split(lax.all_gather(both, axis, axis=dim, tiled=True), ends, axis=along))


def in_blocks(x, dim, length):
    before, after = (x.shape[:dim], x.shape[dim + 1 :])
    return jnp.moveaxis(x.reshape(*before, length, -1, *after), dim, 0)


def sum_at_owner(x, axis, dim):
    length = lax.axis_size(axis)
    tiles = lax.all_to_all(in_blocks(x, dim, length), axis, 0, 0, tiled=True)
    return jnp.sum(tiles.astype(jnp.float32), axis=0)


def sum_by_axis(terms, axes):
    subtotal = terms.astype(jnp.bfloat16)
    for axis in axes:
        subtotal = lax.psum_scatter(subtotal, axis, scatter_dimension=0, tiled=True)
    return subtotal.astype(jnp.float32)


def contract_last(left, right):
    return lax.dot_general(
        left, right, (((1,), (1,)), ((), ())), preferred_element_type=jnp.float32
    )


def body(later_rows, earlier_rows, cotangent, up_weight, down_weight, up_total, down_total):
    rows_dev = later_rows.shape[0]
    total_rows = rows_dev * lax.axis_size(FS) * lax.axis_size("tp")
    factor = 1.0 / math.sqrt(total_rows)
    up_full, down_full = side_by_side((up_weight, down_weight), FS, 0, 1)

    def fetch():
        return (up_full, down_full)

    def to_owner(term):
        return sum_at_owner(term.astype(jnp.bfloat16), "tp", 0)

    def grad_owner(group, right):
        return sum_by_axis(
            lax.dot_general(
                group, right, (((0,), (0,)), ((), ())), preferred_element_type=jnp.float32
            ),
            FS,
        )

    up_whole, down_whole = fetch()
    group = lax.all_gather(later_rows, "tp", axis=0, tiled=True)
    relu_part = jnp.maximum(jnp.dot(group, up_whole, preferred_element_type=jnp.float32), 0.0)
    hidden = (relu_part * relu_part).astype(jnp.bfloat16)
    partial_value = contract_last(hidden, down_whole)
    later_out = to_owner(partial_value).astype(jnp.bfloat16)
    up_whole, down_whole = fetch()
    saved_group, cot_group = side_by_side((earlier_rows, cotangent), "tp", 0, 1)
    relu_part = jnp.maximum(jnp.dot(saved_group, up_whole, preferred_element_type=jnp.float32), 0.0)
    hidden = (relu_part * relu_part).astype(jnp.bfloat16)
    hidden_grad = jnp.dot(cot_group, down_whole, preferred_element_type=jnp.float32)
    pre_grad = (2.0 * relu_part * hidden_grad).astype(jnp.bfloat16)
    input_partial = contract_last(pre_grad, up_whole)
    earlier_grad = to_owner(input_partial).astype(jnp.bfloat16)
    down_updated = down_total + grad_owner(cot_group, hidden) * factor
    up_updated = up_total + grad_owner(saved_group, pre_grad) * factor
    earlier_grad, up_updated, down_updated = (earlier_grad, up_updated, down_updated)
    return (later_out, earlier_grad, up_updated, down_updated)


def solution(mesh):
    finer = Mesh(mesh.devices.reshape(8, 4, mesh.shape["tp"]), ("fs_0", "fs_1", "tp"))
    placed = (
        P(FS_TP, None),
        P(FS_TP, None),
        P(FS_TP, None),
        P(FS, "tp"),
        P(FS, "tp"),
        P(FS, "tp"),
        P(FS, "tp"),
    )
    return jax.shard_map(
        body,
        mesh=finer,
        in_specs=placed,
        out_specs=(P(FS_TP, None), P(FS_TP, None), P(FS, "tp"), P(FS, "tp")),
        check_vma=False,
    )
```

profile of v0, /device:TPU:8, one launch (start us, length us, event | category | flops | bytes accessed | tf_op | source)
XLA Modules:
  0.0 330.6 jit_solution(11753121503092980763)
XLA Ops:
  7.2 0.0 all-gather.4.cloned.1.call-start
  7.2 1.5 pad_maximum_fusion.1
  8.7 0.0 all-gather.4.cloned.1.call-update
  8.8 0.0 all-gather.8.cloned.1.call-start
  8.8 2.3 pad_maximum_fusion
  11.1 0.0 all-gather.8.cloned.1.call-update
  11.1 0.0 all-gather.6.cloned.1.call-start
  11.2 0.7 all-gather.6.cloned.1.call-update
  11.9 0.0 reduce-scatter.9.cloned.1.call-start
  11.9 83.9 %all-gather.4.cloned.1.call-done = bf16[2048,1024]{1,0:T(8,128)(2,1)} async-done(((bf16[64,1024]{1,0:T(8,128)(2,1)}), bf16[2048,1024]{1,0:T(8,128)(2,1)}) %all-gather.4.cloned.1.call-update) | async-done | bytes 4194320 | tf_op jit(solution)/shard_map/all_gather | solution.py:18
  95.8 50.1 %all-gather.8.cloned.1.call-done = bf16[1024,4096]{1,0:T(8,128)(2,1)} async-done(((bf16[128,4096]{1,0:T(8,128)(2,1)}), bf16[1024,4096]{1,0:T(8,128)(2,1)}) %all-gather.8.cloned.1.call-update) | async-done | bytes 8388624 | tf_op jit(solution)/shard_map/all_gather | solution.py:18
  145.9 5.3 %fusion.6 = f32[1024,512]{1,0:T(8,128)S(1)} fusion(bf16[1024,4096]{1,0:T(8,128)(2,1)} %all-gather.8.cloned.1.call-done, bf16[2048,1024]{1,0:T(8,128)(2,1)} %all-gather.4.cloned.1.call-done), kind=kOutput, calls=%fused_computation.8 | convolution fusion | flops 2147483648 | bytes 8388608 | tf_op jit(solution)/shard_map/dot_general | solution.py:73
  151.2 3.7 %fusion.11 = bf16[2048,512]{1,0:T(8,128)(2,1)} fusion(bf16[1024,4096]{1,0:T(8,128)(2,1)S(1)} %copy-done.2, f32[1024,512]{1,0:T(8,128)S(1)} %fusion.6), kind=kOutput, calls=%fused_computation.11 | convolution fusion | flops 2150105088 | bytes 8388608 | tf_op jit(solution)/shard_map/dot_general | solution.py:59
  155.0 27.4 %all-gather.6.cloned.1.call-done = bf16[1024,2048]{1,0:T(8,128)(2,1)} async-done(((bf16[128,2048]{1,0:T(8,128)(2,1)}), bf16[1024,2048]{1,0:T(8,128)(2,1)}) %all-gather.6.cloned.1.call-update) | async-done | bytes 4194320 | tf_op jit(solution)/shard_map/all_gather | solution.py:66
  182.4 10.0 %convolution_convert_fusion.1 = bf16[1024,2048]{1,0:T(8,128)(2,1)} fusion(bf16[2048,1024]{1,0:T(8,128)(2,1)} %all-gather.4.cloned.1.call-done, bf16[1024,2048]{1,0:T(8,128)(2,1)} %all-gather.6.cloned.1.call-done), kind=kOutput, calls=%fused_computation.1 | convolution fusion | flops 4298637312 | bytes 12582912 | tf_op jit(solution)/shard_map/dot_general | solution.py:40
  192.4 6.0 %all-to-all-start = ((bf16[8,128,2048]{2,1,0:T(8,128)(2,1)}), bf16[8,128,2048]{2,1,0:T(8,128)(2,1)}, u32[]{:S(2)}, u32[]{:S(2)}) async-start(bf16[8,128,2048]{2,1,0:T(8,128)(2,1)} %bitcast.6), calls=%async_computation | async-start | bytes 8388608 | tf_op jit(solution)/shard_map/all_to_all | solution.py:28
  198.4 5.2 %multiply_convert_fusion.1 = bf16[1024,512]{1,0:T(8,128)(2,1)S(1)} fusion(f32[1024,512]{1,0:T(8,128)S(1)} %fusion.6, bf16[2048,1024]{1,0:T(8,128)(2,1)} %all-gather.4.cloned.1.call-done, bf16[1024,4096]{1,0:T(8,128)(2,1)} %all-gather.8.cloned.1.call-done), kind=kOutput, calls=%fused_computation.13 | convolution fusion | flops 2149580800 | bytes 9437184 | tf_op jit(solution)/shard_map/dot_general | solution.py:75
  203.6 6.0 %fusion.8 = bf16[2048,512]{1,0:T(8,128)(2,1)} fusion(bf16[1024,512]{1,0:T(8,128)(2,1)S(1)} %multiply_convert_fusion.1, bf16[1024,4096]{1,0:T(8,128)(2,1)} %all-gather.8.cloned.1.call-done), kind=kOutput, calls=%fused_computation.10 | convolution fusion | flops 2148532224 | bytes 7340032 | tf_op jit(solution)/shard_map/dot_general | solution.py:59
  209.5 0.0 reduce-scatter.5.cloned.1.call-update
  209.6 5.9 %convolution_convert_fusion = bf16[1024,2048]{1,0:T(8,128)(2,1)} fusion(bf16[1024,512]{1,0:T(8,128)(2,1)S(1)} %multiply_convert_fusion.1, bf16[2048,1024]{1,0:T(8,128)(2,1)} %all-gather.4.cloned.1.call-done), kind=kOutput, calls=%fused_computation | convolution fusion | flops 2149580800 | bytes 7340032 | tf_op jit(solution)/shard_map/dot_general | solution.py:40
  215.5 31.2 %all-to-all-done = bf16[8,128,2048]{2,1,0:T(8,128)(2,1)} async-done(((bf16[8,128,2048]{2,1,0:T(8,128)(2,1)}), bf16[8,128,2048]{2,1,0:T(8,128)(2,1)}, u32[]{:S(2)}, u32[]{:S(2)}) %all-to-all-start) | async-done | bytes 4194336 | tf_op jit(solution)/shard_map/all_to_all | solution.py:28
  246.7 5.9 %all-to-all-start.1 = ((bf16[8,128,2048]{2,1,0:T(8,128)(2,1)}), bf16[8,128,2048]{2,1,0:T(8,128)(2,1)}, u32[]{:S(2)}, u32[]{:S(2)}) async-start(bf16[8,128,2048]{2,1,0:T(8,128)(2,1)} %bitcast.5), calls=%async_computation.1 | async-start | bytes 8388608 | tf_op jit(solution)/shard_map/all_to_all | solution.py:28
  252.6 0.6 reduce-scatter.11.cloned.1.call-update
  253.2 0.0 reduce-scatter.7.cloned.1.call-start
  253.2 18.8 %reduce-scatter.5.cloned.1.call-done = bf16[256,512]{1,0:T(8,128)(2,1)} async-done(((bf16[2048,512]{1,0:T(8,128)(2,1)}), bf16[256,512]{1,0:T(8,128)(2,1)}) %reduce-scatter.5.cloned.1.call-update) | async-done | bytes 262160 | tf_op jit(solution)/shard_map/reduce_scatter | solution.py:35
  272.0 0.0 reduce-scatter.7.cloned.1.call-update
  272.0 3.9 %reduce_sum.24 = bf16[128,2048]{1,0:T(8,128)(2,1)} reduce(bf16[8,128,2048]{2,1,0:T(8,128)(2,1)} %all-to-all-done, bf16[]{:T(256)} %constant.3.clone.1), dimensions={0}, to_apply=%region_0.0 | reduce | flops 1835008 | bytes 4718594 | tf_op jit(solution)/shard_map/reduce_sum | solution.py:29
  275.9 25.0 %all-to-all-done.1 = bf16[8,128,2048]{2,1,0:T(8,128)(2,1)} async-done(((bf16[8,128,2048]{2,1,0:T(8,128)(2,1)}), bf16[8,128,2048]{2,1,0:T(8,128)(2,1)}, u32[]{:S(2)}, u32[]{:S(2)}) %all-to-all-start.1) | async-done | bytes 4194336 | tf_op jit(solution)/shard_map/all_to_all | solution.py:28
  300.9 3.8 %reduce_sum.25 = bf16[128,2048]{1,0:T(8,128)(2,1)} reduce(bf16[8,128,2048]{2,1,0:T(8,128)(2,1)} %all-to-all-done.1, bf16[]{:T(256)} %constant.3.clone.1), dimensions={0}, to_apply=%region_1.0 | reduce | flops 1835008 | bytes 4718594 | tf_op jit(solution)/shard_map/reduce_sum | solution.py:29
  304.8 1.5 multiply_add_fusion
  306.3 16.0 %reduce-scatter.7.cloned.1.call-done = bf16[64,512]{1,0:T(8,128)(2,1)} async-done(((bf16[256,512]{1,0:T(8,128)(2,1)}), bf16[64,512]{1,0:T(8,128)(2,1)}) %reduce-scatter.7.cloned.1.call-update) | async-done | bytes 65552 | tf_op jit(solution)/shard_map/reduce_scatter | solution.py:35
  322.3 1.5 multiply_add_fusion.1
  (11 shorter events, 0.0 us)
Async XLA Ops:
  7.2 88.6 %all-gather.4.cloned.1.call-start = ((), (), s32[]{:S(2)}) async-start(), calls=%async_computation.6 | async-start | bytes 4325376 | tf_op jit(solution)/shard_map/all_gather | solution.py:18
  8.8 137.1 %all-gather.8.cloned.1.call-start = ((), (), s32[]{:S(2)}) async-start(), calls=%async_computation.8 | async-start | bytes 9437184 | tf_op jit(solution)/shard_map/all_gather | solution.py:18
  11.1 171.2 %all-gather.6.cloned.1.call-start = ((), (), s32[]{:S(2)}) async-start(), calls=%async_computation.7 | async-start | bytes 4718592 | tf_op jit(solution)/shard_map/all_gather | solution.py:66
  11.9 240.7 %reduce-scatter.9.cloned.1.call-start = ((), (), s32[]{:S(2)}) async-start(), calls=%async_computation.11 | async-start | bytes 2359296 | tf_op jit(solution)/shard_map/reduce_scatter | solution.py:35
  145.9 5.3 %copy-start.2 = (bf16[1024,4096]{1,0:T(8,128)(2,1)S(1)}, bf16[1024,4096]{1,0:T(8,128)(2,1)}, u32[]{:S(2)}) copy-start(bf16[1024,4096]{1,0:T(8,128)(2,1)} %all-gather.8.cloned.1.call-done) | copy-start | bytes 25165828
  192.4 54.3 %all-to-all-start = ((bf16[8,128,2048]{2,1,0:T(8,128)(2,1)}), bf16[8,128,2048]{2,1,0:T(8,128)(2,1)}, u32[]{:S(2)}, u32[]{:S(2)}) async-start(bf16[8,128,2048]{2,1,0:T(8,128)(2,1)} %bitcast.6), calls=%async_computation | async-start | bytes 8388608 | tf_op jit(solution)/shard_map/all_to_all | solution.py:28
  198.4 73.6 %reduce-scatter.5.cloned.1.call-start = ((), (), s32[]{:S(2)}) async-start(), calls=%async_computation.9 | async-start | bytes 2359296 | tf_op jit(solution)/shard_map/reduce_scatter | solution.py:35
  246.7 54.2 %all-to-all-start.1 = ((bf16[8,128,2048]{2,1,0:T(8,128)(2,1)}), bf16[8,128,2048]{2,1,0:T(8,128)(2,1)}, u32[]{:S(2)}, u32[]{:S(2)}) async-start(bf16[8,128,2048]{2,1,0:T(8,128)(2,1)} %bitcast.5), calls=%async_computation.1 | async-start | bytes 8388608 | tf_op jit(solution)/shard_map/all_to_all | solution.py:28
  252.6 52.2 %reduce-scatter.11.cloned.1.call-start = ((), (), s32[]{:S(2)}) async-start(), calls=%async_computation.12 | async-start | bytes 327680 | tf_op jit(solution)/shard_map/reduce_scatter | solution.py:35
  253.2 69.1 %reduce-scatter.7.cloned.1.call-start = ((), (), s32[]{:S(2)}) async-start(), calls=%async_computation.10 | async-start | bytes 327680 | tf_op jit(solution)/shard_map/reduce_scatter | solution.py:35
  272.0 32.8 %copy-start = (f32[64,512]{1,0:T(8,128)S(1)}, f32[64,512]{1,0:T(8,128)}, u32[]{:S(2)}) copy-start(f32[64,512]{1,0:T(8,128)} %param.13) | copy-start | bytes 393220
  272.0 50.3 %copy-start.1 = (f32[64,512]{1,0:T(8,128)S(1)}, f32[64,512]{1,0:T(8,128)}, u32[]{:S(2)}) copy-start(f32[64,512]{1,0:T(8,128)} %param.12) | copy-start | bytes 393220
Sparse Core Ops, SparseCore 0:
  11.1 84.6 all-gather.3
  97.6 48.1 all-gather.7
  147.8 34.5 all-gather.5
  184.8 43.4 reduce-scatter.8
  230.7 41.2 reduce-scatter.4
  274.3 22.1 reduce-scatter.10
  299.1 23.1 reduce-scatter.6
where the time goes:
time: 331 us
  waiting for transfers between devices  254 us (77%)
  matrix products  36.1 us (11%)
  other arithmetic  14.6 us (4%)
  between operations  14.2 us (4%)
  starting transfers between devices  12.1 us (4%)
    all_gather x2, waiting for transfers between devices, side_by_side(): lax.all_gather(both, axis, axis=dim, tiled=True)  134 us
    all_to_all x2, waiting for transfers between devices, sum_at_owner(): tiles = lax.all_to_all(in_blocks(x, dim, length), axis, 0, 0, tiled=True)  56.2 us
    reduce_scatter x4, waiting for transfers between devices, sum_by_axis(): subtotal = lax.psum_scatter(subtotal, axis, scatter_dimension=0, tiled=True)  34.8 us
    all_gather x1, waiting for transfers between devices, body(): group = lax.all_gather(later_rows, 'tp', axis=0, tiled=True)  27.4 us
    dot_general x2, matrix products, contract_last(): lax.dot_general(left, right, (((1,), (1,)), ((), ())), preferred_element_...  15.9 us
    all_to_all x2, starting transfers between devices, sum_at_owner(): tiles = lax.all_to_all(in_blocks(x, dim, length), axis, 0, 0, tiled=True)  11.9 us
    dot_general x2, matrix products, grad_owner(): lax.dot_general(group, right, (((0,), (0,)), ((), ())), preferred_element...  9.68 us
    reduce_sum x2, other arithmetic, sum_at_owner(): return jnp.sum(tiles.astype(jnp.float32), axis=0)  7.73 us
  transfers between devices with their start and end apart: 9, of which 7 were waited for; matrix products, arithmetic and copies ran while one was open for 14% of the time, Pallas kernels for 0%

commit v1 on v0

--- a/solution.py
+++ b/solution.py
@@ -7,6 +7,27 @@
 
 FS = ("fs_0", "fs_1")
 FS_TP = ("fs_0", "fs_1", "tp")
+
+
+def collect(x, axis, dim):
+    size, position, rows = (lax.axis_size(axis), lax.axis_index(axis), x.shape[dim])
+    right = [(i, (i + 1) % size) for i in range(size)]
+    behind = [(i, (i - 1) % size) for i in range(size)]
+    out = jnp.zeros((*x.shape[:dim], size * rows, *x.shape[dim + 1 :]), x.dtype)
+    out = lax.dynamic_update_slice_in_dim(out, x, position * rows, axis=dim)
+    from_left = from_right = x
+    middle = size // 2
+    for step in range(1, middle + 1):
+        from_left = lax.ppermute(from_left, axis, right)
+        out = lax.dynamic_update_slice_in_dim(
+            out, from_left, (position - step) % size * rows, axis=dim
+        )
+        if step < size - middle:
+            from_right = lax.ppermute(from_right, axis, behind)
+            out = lax.dynamic_update_slice_in_dim(
+                out, from_right, (position + step) % size * rows, axis=dim
+            )
+    return out
 
 
 def side_by_side(arrays, axis, dim, along):
@@ -63,7 +84,7 @@
         )
 
     up_whole, down_whole = fetch()
-    group = lax.all_gather(later_rows, "tp", axis=0, tiled=True)
+    group = collect(later_rows, "tp", 0)
     relu_part = jnp.maximum(jnp.dot(group, up_whole, preferred_element_type=jnp.float32), 0.0)
     hidden = (relu_part * relu_part).astype(jnp.bfloat16)
     partial_value = contract_last(hidden, down_whole)

time: 331 us -> 306 us (0.924)
  waiting for transfers between devices: 254 us -> 214 us
  local copies, waits for them, and re-layouts: 0.02 us -> 11.5 us
  starting transfers between devices: 12.1 us -> 17.6 us
    all_gather x1 -> x0, waiting for transfers between devices: 27.4 us -> none  [body(): group = lax.all_gather(later_rows, 'tp', axis=0, tiled=True)]
    all_gather x2, waiting for transfers between devices: 134 us -> 109 us  [side_by_side(): lax.all_gather(both, axis, axis=dim, tiled=True)]
    ppermute x0 -> x7, waiting for transfers between devices: none -> 14.6 us  [the longest x4 14.6 us: collect(): from_left = lax.ppermute(from_left, axis, right)]
    reduce_scatter x4, waiting for transfers between devices: 34.8 us -> 23.7 us  [sum_by_axis(): subtotal = lax.psum_scatter(subtotal, axis, scatter_dimension=0, tiled=True)]
    all_to_all x2, waiting for transfers between devices: 56.2 us -> 66.7 us  [sum_at_owner(): tiles = lax.all_to_all(in_blocks(x, dim, length), axis, 0, 0, tiled=True)]
    dynamic_update_slice x0 -> x8, local copies, waits for them, and re-layouts: none -> 6.84 us  [the longest x4 3.44 us: collect(): lax.dynamic_update_slice_in_dim(out, from_left, (position - step) % size...]
    ppermute x0 -> x7, starting transfers between devices: none -> 5.54 us  [the longest x3 5.52 us: collect(): from_right = lax.ppermute(from_right, axis, behind)]
  transfers between devices with their start and end apart: 9 -> 15, of which waited for: 7 -> 9; matrix products, arithmetic and copies ran while one was open for 14% -> 18% of each run, Pallas kernels for 0% -> 0%
where the time goes in v1:
time: 306 us; the launch traced here: 305 us
  waiting for transfers between devices  214 us (70%)
  matrix products  33.2 us (11%)
  starting transfers between devices  17.6 us (6%)
  other arithmetic  14.6 us (5%)
  between operations  14.2 us (5%)
  local copies, waits for them, and re-layouts  11.5 us (4%)
    all_gather x2, waiting for transfers between devices, side_by_side(): lax.all_gather(both, axis, axis=dim, tiled=True)  109 us
    all_to_all x2, waiting for transfers between devices, sum_at_owner(): tiles = lax.all_to_all(in_blocks(x, dim, length), axis, 0, 0, tiled=True)  66.7 us
    reduce_scatter x4, waiting for transfers between devices, sum_by_axis(): subtotal = lax.psum_scatter(subtotal, axis, scatter_dimension=0, tiled=True)  23.7 us
    dot_general x2, matrix products, contract_last(): lax.dot_general(left, right, (((1,), (1,)), ((), ())), preferred_element_...  15.8 us
    ppermute x4, waiting for transfers between devices, collect(): from_left = lax.ppermute(from_left, axis, right)  14.6 us
    all_to_all x2, starting transfers between devices, sum_at_owner(): tiles = lax.all_to_all(in_blocks(x, dim, length), axis, 0, 0, tiled=True)  11.9 us
    dot_general x2, matrix products, grad_owner(): lax.dot_general(group, right, (((0,), (0,)), ((), ())), preferred_element...  9.77 us
    reduce_sum x2, other arithmetic, sum_at_owner(): return jnp.sum(tiles.astype(jnp.float32), axis=0)  7.73 us
  transfers between devices with their start and end apart: 15, of which 9 were waited for; matrix products, arithmetic and copies ran while one was open for 18% of the time, Pallas kernels for 0%

profile of v1, /device:TPU:8, one launch (start us, length us, event | category | flops | bytes accessed | tf_op | source)
XLA Modules:
  0.0 305.4 jit_solution(14399257976602891786)
XLA Ops:
  7.2 1.6 pad_maximum_fusion.1
  8.9 2.3 pad_maximum_fusion
  11.3 1.7 collective-permute-start.1
  13.0 7.1 %collective-permute-done = bf16[128,2048]{1,0:T(8,128)(2,1)S(1)} collective-permute-done((bf16[128,2048]{1,0:T(8,128)(2,1)}, bf16[128,2048]{1,0:T(8,128)(2,1)S(1)}, u32[]{:S(2)}, u32[]{:S(2)}) %collective-permute-start) | collective-permute-done | bytes 524320 | tf_op jit(solution)/shard_map/ppermute | solution.py:21
  20.1 2.0 collective-permute-start.3
  22.1 2.5 broadcast_in_dim.3
  25.4 3.3 %collective-permute-done.2 = bf16[128,2048]{1,0:T(8,128)(2,1)S(1)} collective-permute-done((bf16[128,2048]{1,0:T(8,128)(2,1)S(1)}, bf16[128,2048]{1,0:T(8,128)(2,1)S(1)}, u32[]{:S(2)}, u32[]{:S(2)}) %collective-permute-start.2) | collective-permute-done | bytes 524320 | tf_op jit(solution)/shard_map/ppermute | solution.py:21
  28.7 0.9 constant_dynamic-update-slice_fusion.6
  29.6 0.9 constant_dynamic-update-slice_fusion.5
  30.4 1.8 collective-permute-start.5
  32.2 0.9 constant_dynamic-update-slice_fusion.4
  33.0 4.2 %collective-permute-done.4 = bf16[128,2048]{1,0:T(8,128)(2,1)S(1)} collective-permute-done((bf16[128,2048]{1,0:T(8,128)(2,1)S(1)}, bf16[128,2048]{1,0:T(8,128)(2,1)S(1)}, u32[]{:S(2)}, u32[]{:S(2)}) %collective-permute-start.4) | collective-permute-done | bytes 524320 | tf_op jit(solution)/shard_map/ppermute | solution.py:21
  37.3 58.6 %all-gather.3.cloned.1.call-done = bf16[2048,1024]{1,0:T(8,128)(2,1)} async-done(((bf16[64,1024]{1,0:T(8,128)(2,1)}), bf16[2048,1024]{1,0:T(8,128)(2,1)}) %all-gather.3.cloned.1.call-update) | async-done | bytes 4194320 | tf_op jit(solution)/shard_map/all_gather | solution.py:39
  95.9 50.1 %all-gather.5.cloned.1.call-done = bf16[1024,4096]{1,0:T(8,128)(2,1)} async-done(((bf16[128,4096]{1,0:T(8,128)(2,1)}), bf16[1024,4096]{1,0:T(8,128)(2,1)}) %all-gather.5.cloned.1.call-update) | async-done | bytes 8388624 | tf_op jit(solution)/shard_map/all_gather | solution.py:39
  146.0 5.3 %fusion.6 = f32[1024,512]{1,0:T(8,128)S(1)} fusion(bf16[1024,4096]{1,0:T(8,128)(2,1)} %all-gather.5.cloned.1.call-done, bf16[2048,1024]{1,0:T(8,128)(2,1)} %all-gather.3.cloned.1.call-done), kind=kOutput, calls=%fused_computation.8 | convolution fusion | flops 2147483648 | bytes 8388608 | tf_op jit(solution)/shard_map/dot_general | solution.py:94
  151.3 1.1 copy-done.4
  152.4 2.3 multiply_convert_fusion.1
  154.8 1.1 copy-done.7
  155.8 3.7 %fusion.8 = bf16[2048,512]{1,0:T(8,128)(2,1)} fusion(bf16[1024,512]{1,0:T(8,128)(2,1)S(1)} %multiply_convert_fusion.1, bf16[1024,4096]{1,0:T(8,128)(2,1)S(1)} %copy-done.3), kind=kOutput, calls=%fused_computation.10 | convolution fusion | flops 2148532224 | bytes 7340032 | tf_op jit(solution)/shard_map/dot_general | solution.py:80
  163.0 9.9 %convolution_convert_fusion.1 = bf16[1024,2048]{1,0:T(8,128)(2,1)} fusion(bf16[2048,1024]{1,0:T(8,128)(2,1)} %all-gather.3.cloned.1.call-done, bf16[1024,2048]{1,0:T(8,128)(2,1)} %constant_dynamic-update-slice_fusion), kind=kOutput, calls=%fused_computation.1 | convolution fusion | flops 4298637312 | bytes 12582912 | tf_op jit(solution)/shard_map/dot_general | solution.py:61
  172.9 6.0 %all-to-all-start = ((bf16[8,128,2048]{2,1,0:T(8,128)(2,1)}), bf16[8,128,2048]{2,1,0:T(8,128)(2,1)}, u32[]{:S(2)}, u32[]{:S(2)}) async-start(bf16[8,128,2048]{2,1,0:T(8,128)(2,1)} %bitcast.6), calls=%async_computation | async-start | bytes 8388608 | tf_op jit(solution)/shard_map/all_to_all | solution.py:49
  178.9 6.0 %fusion.11 = bf16[2048,512]{1,0:T(8,128)(2,1)} fusion(bf16[1024,4096]{1,0:T(8,128)(2,1)} %all-gather.5.cloned.1.call-done, f32[1024,512]{1,0:T(8,128)S(1)} %copy-done.6), kind=kOutput, calls=%fused_computation.11 | convolution fusion | flops 2150105088 | bytes 8388608 | tf_op jit(solution)/shard_map/dot_general | solution.py:80
  184.9 5.9 %convolution_convert_fusion = bf16[1024,2048]{1,0:T(8,128)(2,1)} fusion(bf16[1024,512]{1,0:T(8,128)(2,1)S(1)} %copy-done.8, bf16[2048,1024]{1,0:T(8,128)(2,1)} %all-gather.3.cloned.1.call-done), kind=kOutput, calls=%fused_computation | convolution fusion | flops 2149580800 | bytes 7340032 | tf_op jit(solution)/shard_map/dot_general | solution.py:61
  190.9 36.3 %all-to-all-done = bf16[8,128,2048]{2,1,0:T(8,128)(2,1)} async-done(((bf16[8,128,2048]{2,1,0:T(8,128)(2,1)}), bf16[8,128,2048]{2,1,0:T(8,128)(2,1)}, u32[]{:S(2)}, u32[]{:S(2)}) %all-to-all-start) | async-done | bytes 4194336 | tf_op jit(solution)/shard_map/all_to_all | solution.py:49
  227.2 5.9 %all-to-all-start.1 = ((bf16[8,128,2048]{2,1,0:T(8,128)(2,1)}), bf16[8,128,2048]{2,1,0:T(8,128)(2,1)}, u32[]{:S(2)}, u32[]{:S(2)}) async-start(bf16[8,128,2048]{2,1,0:T(8,128)(2,1)} %bitcast.5), calls=%async_computation.1 | async-start | bytes 8388608 | tf_op jit(solution)/shard_map/all_to_all | solution.py:49
  233.7 13.4 %reduce-scatter.9.cloned.1.call-done = bf16[256,512]{1,0:T(8,128)(2,1)} async-done(((bf16[2048,512]{1,0:T(8,128)(2,1)}), bf16[256,512]{1,0:T(8,128)(2,1)}) %reduce-scatter.9.cloned.1.call-update) | async-done | bytes 262160 | tf_op jit(solution)/shard_map/reduce_scatter | solution.py:56
  247.1 3.9 %reduce_sum.24 = bf16[128,2048]{1,0:T(8,128)(2,1)} reduce(bf16[8,128,2048]{2,1,0:T(8,128)(2,1)} %all-to-all-done, bf16[]{:T(256)} %constant.55.clone.1), dimensions={0}, to_apply=%region_0.1 | reduce | flops 1835008 | bytes 4718594 | tf_op jit(solution)/shard_map/reduce_sum | solution.py:50
  251.0 30.4 %all-to-all-done.1 = bf16[8,128,2048]{2,1,0:T(8,128)(2,1)} async-done(((bf16[8,128,2048]{2,1,0:T(8,128)(2,1)}), bf16[8,128,2048]{2,1,0:T(8,128)(2,1)}, u32[]{:S(2)}, u32[]{:S(2)}) %all-to-all-start.1) | async-done | bytes 4194336 | tf_op jit(solution)/shard_map/all_to_all | solution.py:49
  281.4 3.8 %reduce_sum.25 = bf16[128,2048]{1,0:T(8,128)(2,1)} reduce(bf16[8,128,2048]{2,1,0:T(8,128)(2,1)} %all-to-all-done.1, bf16[]{:T(256)} %constant.55.clone.1), dimensions={0}, to_apply=%region_1.2 | reduce | flops 1835008 | bytes 4718594 | tf_op jit(solution)/shard_map/reduce_sum | solution.py:50
  285.2 1.5 multiply_add_fusion.1
  286.7 10.3 %reduce-scatter.11.cloned.1.call-done = bf16[64,512]{1,0:T(8,128)(2,1)} async-done(((bf16[256,512]{1,0:T(8,128)(2,1)}), bf16[64,512]{1,0:T(8,128)(2,1)}) %reduce-scatter.11.cloned.1.call-update) | async-done | bytes 65552 | tf_op jit(solution)/shard_map/reduce_scatter | solution.py:56
  297.0 1.5 multiply_add_fusion
  (43 shorter events, 5.1 us)
Async XLA Ops:
  7.2 17.4 %copy-start = (bf16[128,2048]{1,0:T(8,128)(2,1)S(1)}, bf16[128,2048]{1,0:T(8,128)(2,1)}, u32[]{:S(2)}) copy-start(bf16[128,2048]{1,0:T(8,128)(2,1)} %param.7) | copy-start | bytes 1572868
  7.2 88.7 %all-gather.3.cloned.1.call-start = ((), (), s32[]{:S(2)}) async-start(), calls=%async_computation.6 | async-start | bytes 4325376 | tf_op jit(solution)/shard_map/all_gather | solution.py:39
  8.8 137.1 %all-gather.5.cloned.1.call-start = ((), (), s32[]{:S(2)}) async-start(), calls=%async_computation.7 | async-start | bytes 9437184 | tf_op jit(solution)/shard_map/all_gather | solution.py:39
  11.2 221.9 %reduce-scatter.5.cloned.1.call-start = ((), (), s32[]{:S(2)}) async-start(), calls=%async_computation.8 | async-start | bytes 2359296 | tf_op jit(solution)/shard_map/reduce_scatter | solution.py:56
  11.2 8.8 %collective-permute-start = (bf16[128,2048]{1,0:T(8,128)(2,1)}, bf16[128,2048]{1,0:T(8,128)(2,1)S(1)}, u32[]{:S(2)}, u32[]{:S(2)}) collective-permute-start(bf16[128,2048]{1,0:T(8,128)(2,1)} %param.7), channel_id=1, source_target_pairs={{0,1},{1,2},{2,3},{3,4},{4,5},{5,6},{6,7},{7,0},{8,9},{9,10},{10,1... | collective-permute-start | bytes 1572872 | tf_op jit(solution)/shard_map/ppermute | solution.py:21
  11.3 8.8 %collective-permute-start.1 = (bf16[128,2048]{1,0:T(8,128)(2,1)}, bf16[128,2048]{1,0:T(8,128)(2,1)S(1)}, u32[]{:S(2)}, u32[]{:S(2)}) collective-permute-start(bf16[128,2048]{1,0:T(8,128)(2,1)} %param.7), channel_id=1, source_target_pairs={{0,7},{1,0},{2,1},{3,2},{4,3},{5,4},{6,5},{7,6},{8,15},{9,8},{10,9... | collective-permute-start | bytes 1572872 | tf_op jit(solution)/shard_map/ppermute | solution.py:26
  20.1 8.6 %collective-permute-start.2 = (bf16[128,2048]{1,0:T(8,128)(2,1)S(1)}, bf16[128,2048]{1,0:T(8,128)(2,1)S(1)}, u32[]{:S(2)}, u32[]{:S(2)}) collective-permute-start(bf16[128,2048]{1,0:T(8,128)(2,1)S(1)} %collective-permute-done), channel_id=1, source_target_pairs={{0,1},{1,2},{2,3},{3,4},{4,5},{5,6},{6,7},{7,0},{8,9},{9,10},{10,1... | collective-permute-start | bytes 1572872 | tf_op jit(solution)/shard_map/ppermute | solution.py:21
  20.1 10.3 %collective-permute-start.3 = (bf16[128,2048]{1,0:T(8,128)(2,1)S(1)}, bf16[128,2048]{1,0:T(8,128)(2,1)S(1)}, u32[]{:S(2)}, u32[]{:S(2)}) collective-permute-start(bf16[128,2048]{1,0:T(8,128)(2,1)S(1)} %collective-permute-done.1), channel_id=1, source_target_pairs={{0,7},{1,0},{2,1},{3,2},{4,3},{5,4},{6,5},{7,6},{8,15},{9,8},{10,9... | collective-permute-start | bytes 1572872 | tf_op jit(solution)/shard_map/ppermute | solution.py:26
  28.7 8.6 %collective-permute-start.4 = (bf16[128,2048]{1,0:T(8,128)(2,1)S(1)}, bf16[128,2048]{1,0:T(8,128)(2,1)S(1)}, u32[]{:S(2)}, u32[]{:S(2)}) collective-permute-start(bf16[128,2048]{1,0:T(8,128)(2,1)S(1)} %collective-permute-done.2), channel_id=1, source_target_pairs={{0,1},{1,2},{2,3},{3,4},{4,5},{5,6},{6,7},{7,0},{8,9},{9,10},{10,1... | collective-permute-start | bytes 1572872 | tf_op jit(solution)/shard_map/ppermute | solution.py:21
  30.4 130.9 %collective-permute-start.5 = (bf16[128,2048]{1,0:T(8,128)(2,1)S(1)}, bf16[128,2048]{1,0:T(8,128)(2,1)S(1)}, u32[]{:S(2)}, u32[]{:S(2)}) collective-permute-start(bf16[128,2048]{1,0:T(8,128)(2,1)S(1)} %collective-permute-done.3), channel_id=1, source_target_pairs={{0,7},{1,0},{2,1},{3,2},{4,3},{5,4},{6,5},{7,6},{8,15},{9,8},{10,9... | collective-permute-start | bytes 1572872 | tf_op jit(solution)/shard_map/ppermute | solution.py:26
  37.3 124.9 %collective-permute-start.6 = (bf16[128,2048]{1,0:T(8,128)(2,1)S(1)}, bf16[128,2048]{1,0:T(8,128)(2,1)S(1)}, u32[]{:S(2)}, u32[]{:S(2)}) collective-permute-start(bf16[128,2048]{1,0:T(8,128)(2,1)S(1)} %collective-permute-done.4), channel_id=1, source_target_pairs={{0,1},{1,2},{2,3},{3,4},{4,5},{5,6},{6,7},{7,0},{8,9},{9,10},{10,1... | collective-permute-start | bytes 1572872 | tf_op jit(solution)/shard_map/ppermute | solution.py:21
  146.0 5.3 %copy-start.3 = (bf16[1024,4096]{1,0:T(8,128)(2,1)S(1)}, bf16[1024,4096]{1,0:T(8,128)(2,1)}, u32[]{:S(2)}) copy-start(bf16[1024,4096]{1,0:T(8,128)(2,1)} %all-gather.5.cloned.1.call-done) | copy-start | bytes 25165828
  146.0 6.4 %copy-start.4 = (bf16[2048,1024]{1,0:T(8,128)(2,1)S(1)}, bf16[2048,1024]{1,0:T(8,128)(2,1)}, u32[]{:S(2)}) copy-start(bf16[2048,1024]{1,0:T(8,128)(2,1)} %all-gather.3.cloned.1.call-done) | copy-start | bytes 12582916
  152.4 2.3 copy-start.5
  154.8 1.1 copy-start.7
  172.9 6.0 %copy-start.6 = (f32[1024,512]{1,0:T(8,128)S(1)}, f32[1024,512]{1,0:T(8,128)}, u32[]{:S(2)}) copy-start(f32[1024,512]{1,0:T(8,128)} %copy-done.5) | copy-start | bytes 6291460
  172.9 54.3 %all-to-all-start = ((bf16[8,128,2048]{2,1,0:T(8,128)(2,1)}), bf16[8,128,2048]{2,1,0:T(8,128)(2,1)}, u32[]{:S(2)}, u32[]{:S(2)}) async-start(bf16[8,128,2048]{2,1,0:T(8,128)(2,1)} %bitcast.6), calls=%async_computation | async-start | bytes 8388608 | tf_op jit(solution)/shard_map/all_to_all | solution.py:49
  178.8 6.1 %copy-start.8 = (bf16[1024,512]{1,0:T(8,128)(2,1)S(1)}, bf16[1024,512]{1,0:T(8,128)(2,1)}, u32[]{:S(2)}) copy-start(bf16[1024,512]{1,0:T(8,128)(2,1)} %copy-done.7) | copy-start | bytes 3145732
  178.8 68.2 %reduce-scatter.9.cloned.1.call-start = ((), (), s32[]{:S(2)}) async-start(), calls=%async_computation.10 | async-start | bytes 2359296 | tf_op jit(solution)/shard_map/reduce_scatter | solution.py:56
  227.2 54.2 %all-to-all-start.1 = ((bf16[8,128,2048]{2,1,0:T(8,128)(2,1)}), bf16[8,128,2048]{2,1,0:T(8,128)(2,1)}, u32[]{:S(2)}, u32[]{:S(2)}) async-start(bf16[8,128,2048]{2,1,0:T(8,128)(2,1)} %bitcast.5), calls=%async_computation.1 | async-start | bytes 8388608 | tf_op jit(solution)/shard_map/all_to_all | solution.py:49
  233.1 52.2 %reduce-scatter.7.cloned.1.call-start = ((), (), s32[]{:S(2)}) async-start(), calls=%async_computation.9 | async-start | bytes 327680 | tf_op jit(solution)/shard_map/reduce_scatter | solution.py:56
  233.6 63.4 %reduce-scatter.11.cloned.1.call-start = ((), (), s32[]{:S(2)}) async-start(), calls=%async_computation.11 | async-start | bytes 327680 | tf_op jit(solution)/shard_map/reduce_scatter | solution.py:56
  247.1 38.1 %copy-start.1 = (f32[64,512]{1,0:T(8,128)S(1)}, f32[64,512]{1,0:T(8,128)}, u32[]{:S(2)}) copy-start(f32[64,512]{1,0:T(8,128)} %param.12) | copy-start | bytes 393220
  247.1 49.9 %copy-start.2 = (f32[64,512]{1,0:T(8,128)S(1)}, f32[64,512]{1,0:T(8,128)}, u32[]{:S(2)}) copy-start(f32[64,512]{1,0:T(8,128)} %param.13) | copy-start | bytes 393220
Sparse Core Ops, SparseCore 0:
  11.1 84.6 all-gather.2
  97.7 48.1 all-gather.4
  159.7 43.8 reduce-scatter.4
  206.0 41.0 reduce-scatter.8
  249.4 22.0 reduce-scatter.6
  273.9 23.1 reduce-scatter.10
